TPU v7x, 512 devices: a whole 4x8x8 slice. The times are simulated.
512 devices in a mesh: ep: 32 (over z, x), tp: 16 (over y, core).
Axes of the slice: x: 4, y: 8, z: 8, core: 2. Of those that a mesh axis runs over, the one named last changes fastest.
Arguments:
- mix_input: bfloat16 [16384, 2048], P('ep', 'tp'), may hold values from -6 to 6
- mix_weight: bfloat16 [2048, 4096], P(None, 'tp'), may hold values from -0.125 to 0.125
- expert_input: bfloat16 [4096, 4096], P('ep', 'tp'), may hold values from -4500 to 4500
- expert_index: int32 [4096, 2], P('ep'), may hold values from 0 to 31, as said below
- route_share: float32 [4096, 2], P('ep'), may hold values from 0.1 to 1
- norm_gain: float32 [4096], replicated, may hold values from 0.1 to 1.9
- gate_weight: bfloat16 [32, 4096, 2048], P('ep', None, 'tp'), may hold values from -0.09375 to 0.09375
- up_weight: bfloat16 [32, 4096, 2048], P('ep', None, 'tp'), may hold values from -0.09375 to 0.09375
- down_weight: bfloat16 [32, 2048, 4096], P('ep', None, 'tp'), may hold values from -0.125 to 0.125
Outputs:
- mixed_rows: bfloat16 [16384, 4096], P('ep', 'tp')
- expert_rows: bfloat16 [4096, 4096], P('ep', 'tp')
Inputs may be any that keep to these rules, and one draw needn't show every extreme that they name: `expert_index`: each row names 2 different experts. Within each aligned block of 128 rows (the rows of one index of ep) no expert is named by more than 16 rows, and one expert, the same in every block, is named by exactly 16 rows.
All inputs are finite; a program needn't handle non-finite values.
Results may differ from a plain program's by a relative error of at most 0.007.
Values may be sent and summed in bfloat16 or wider, within the bound.
A program may use at most 64 MiB of HBM per device.

v0:
```python
import jax
import jax.numpy as jnp
from jax import lax
from jax.sharding import PartitionSpec as P

POOL = 2048
TOP = 2


window_reach = 15
norm_eps = 1e-06


def passed_along(value, axis, by):
    size = lax.axis_size(axis)
    pairs = [(i, i + by) for i in range(size) if 0 <= i + by < size]
    return lax.ppermute(value, axis, pairs)


def laid_out(parts, dim):
    lengths = list(parts.shape[1:])
    lengths[dim] *= parts.shape[0]
    return jnp.moveaxis(parts, 0, dim).reshape(lengths)


def copy_for_each(value, axis):
    size = lax.axis_size(axis)
    return lax.all_to_all(
        jnp.broadcast_to(value[None], (size, *value.shape)), axis, 0, 0, tiled=True
    )


def gathered_copies(value, axis, dim):
    return laid_out(copy_for_each(value, axis), dim)


def pool_minus_self(extended, first_pos, group_size, channel_base):
    length = extended.shape[0] - window_reach
    channels = extended.shape[1]
    channel = channel_base + jnp.arange(channels, dtype=jnp.int32)
    window = jnp.power(2, channel // group_size + 1).astype(jnp.int32)
    running = jnp.zeros((length, channels), jnp.float32)
    for lag_count in range(window_reach + 1):
        shifted = extended[window_reach - lag_count : window_reach - lag_count + length]
        running = running + jnp.where(lag_count < window[None, :], shifted, 0.0)
    position = first_pos + jnp.arange(length, dtype=jnp.int32)
    counts = jnp.minimum(position[:, None] + 1, window[None, :]).astype(jnp.float32)
    return (running / counts - extended[window_reach:]).astype(jnp.bfloat16)


def slot_targets(indices, experts, capacity):
    flattened = indices.reshape(-1)
    one_hot = (flattened[:, None] == jnp.arange(experts, dtype=jnp.int32)[None, :]).astype(
        jnp.int32
    )
    earlier = jnp.cumsum(one_hot, axis=0) - one_hot
    return flattened * capacity + jnp.sum(earlier * one_hot, axis=1)


def shards(
    mix_input,
    mix_weight,
    expert_input,
    expert_index,
    route_share,
    norm_gain,
    gate_weight,
    up_weight,
    down_weight,
):
    tokens_mix, channels = mix_input.shape
    trailing = mix_input[tokens_mix - window_reach :]
    previous = passed_along(trailing, "ep", 1)
    extended = jnp.concatenate([previous, mix_input], axis=0).astype(jnp.float32)
    pooled = pool_minus_self(
        extended, lax.axis_index("ep") * tokens_mix, POOL // 4, lax.axis_index("tp") * channels
    )
    mixed_rows = jnp.dot(
        lax.all_gather(pooled, "tp", axis=1, tiled=True),
        mix_weight,
        preferred_element_type=jnp.float32,
    ).astype(jnp.bfloat16)
    tokens_exp = expert_input.shape[0]
    local_experts = gate_weight.shape[0]
    experts = local_experts * lax.axis_size("ep")
    capacity = 2 * tokens_exp * TOP // experts
    model_width = norm_gain.shape[0]
    targets = slot_targets(expert_index, experts, capacity)
    sources = jnp.repeat(jnp.arange(tokens_exp, dtype=jnp.int32), TOP)
    table = jnp.full((experts * capacity,), tokens_exp, jnp.int32).at[targets].set(sources)
    feature_block = expert_input.shape[1]
    padded = jnp.concatenate([expert_input, jnp.zeros((1, feature_block), jnp.bfloat16)], axis=0)
    outgoing = padded[table].reshape(experts, capacity, feature_block)
    arrived = lax.all_to_all(outgoing, "ep", split_axis=0, concat_axis=1, tiled=True)
    portion = lax.all_gather(arrived, "tp", axis=2, tiled=True)
    scaled = (portion.astype(jnp.float32) * norm_gain).astype(jnp.bfloat16)
    gate_acts = jnp.einsum("erd,edh->erh", scaled, gate_weight, preferred_element_type=jnp.float32)
    up_acts = jnp.einsum("erd,edh->erh", scaled, up_weight, preferred_element_type=jnp.float32)
    squares = jnp.sum(jnp.square(portion.astype(jnp.float32)), axis=2)
    inverse = lax.rsqrt(squares / model_width + norm_eps)[:, :, None]
    hidden = (jax.nn.silu(gate_acts * inverse) * (up_acts * inverse)).astype(jnp.bfloat16)
    produced = jnp.einsum(
        "erh,ehc->erc",
        gathered_copies(hidden, "tp", 2),
        down_weight,
        preferred_element_type=jnp.float32,
    ).astype(jnp.bfloat16)
    returned = lax.all_to_all(produced, "ep", split_axis=1, concat_axis=0, tiled=True)
    returned = returned.reshape(experts * capacity, returned.shape[2])
    picked = returned[targets].astype(jnp.float32).reshape(tokens_exp, TOP, returned.shape[1])
    shares = route_share / jnp.sum(route_share, axis=1, keepdims=True)
    expert_rows = jnp.sum(picked * shares[:, :, None], axis=1).astype(jnp.bfloat16)
    return (mixed_rows, expert_rows)


def solution(mesh):
    placed = (
        P("ep", "tp"),
        P(None, "tp"),
        P("ep", "tp"),
        P("ep", None),
        P("ep", None),
        P(),
        P("ep", None, "tp"),
        P("ep", None, "tp"),
        P("ep", None, "tp"),
    )
    return jax.shard_map(
        shards,
        mesh=mesh,
        in_specs=placed,
        out_specs=(P("ep", "tp"), P("ep", "tp")),
        check_vma=False,
    )
```

profile of v0, /device:TPU:1, one launch (start us, length us, event | category | flops | bytes accessed | tf_op | source)
XLA Modules:
  0.0 190.6 jit_solution(15322384750593228259)
XLA Ops:
  7.2 0.0 copy-start
  7.2 0.0 copy-start.6
  7.2 0.0 all-gather.5.cloned.1.call-start
  7.2 0.8 broadcast_multiply_fusion
  8.1 0.8 copy.27
  8.8 0.1 eq.29
  9.0 0.1 eq.25
  9.1 0.1 copy.26
  9.2 0.1 mul.314
  9.4 0.6 reduce-window.6
  10.0 0.2 slice_reduce_fusion
  10.2 0.1 reshape.270
  10.4 0.1 fusion.43
  10.5 1.4 scatter_custom_fusion
  11.9 0.8 concatenate.7
  12.8 1.9 %gather_fusion = bf16[512,256]{1,0:T(8,128)(2,1)S(1)} fusion(bf16[129,256]{1,0:T(8,128)(2,1)S(1)} %concatenate.7, s32[1024]{0:T(1024)S(1)} %pad_clamp_fusion.1), kind=kCustom, calls=%fused_computation | custom fusion | bytes 526336 | tf_op jit(solution)/shard_map/gather | solution.py:93
  14.7 24.9 %all_to_all.26 = bf16[32,16,256]{2,1,0:T(8,128)(2,1)} all-to-all(bf16[32,16,256]{2,1,0:T(8,128)(2,1)S(1)} %bitcast.67), channel_id=1, replica_groups=mesh['ep'=32,'tp'=16] {'ep'}, dimensions={0} | all-to-all | bytes 524288 | tf_op jit(solution)/shard_map/all_to_all | solution.py:94
  39.6 0.0 all-gather.5.cloned.1.call-update
  39.7 0.7 slice.58
  40.4 2.1 %collective-permute-start = (bf16[15,128]{1,0:T(8,128)(2,1)S(1)}, bf16[15,128]{1,0:T(8,128)(2,1)S(1)}, u32[]{:S(2)}, u32[]{:S(2)}) collective-permute-start(bf16[15,128]{1,0:T(8,128)(2,1)S(1)} %slice.58), channel_id=1, source_target_pairs={{0,16},{16,32},{32,48},{48,64},{64,80},{80,96},{96,112},{112,128},... | collective-permute-start | bytes 11528 | tf_op jit(solution)/shard_map/ppermute | solution.py:17
  42.7 47.3 %all-gather.5.cloned.1.call-done = bf16[1,512,4096]{2,1,0:T(8,128)(2,1)} async-done(((bf16[1,512,256]{2,1,0:T(8,128)(2,1)}), bf16[1,512,4096]{2,1,0:T(8,128)(2,1)}) %all-gather.5.cloned.1.call-update) | async-done | bytes 4194320 | tf_op jit(solution)/shard_map/all_gather | solution.py:95
  90.0 3.2 %fusion.1 = f32[512]{0:T(512)S(1)} fusion(bf16[1,512,4096]{2,1,0:T(8,128)(2,1)} %all-gather.5.cloned.1.call-done), kind=kLoop, calls=%fused_computation.6 | loop fusion | flops 6290944 | bytes 4196352 | tf_op jit(solution)/shard_map/reduce_sum | solution.py:99
  93.3 0.2 copy-done.1
  93.4 1.3 fusion.8
  94.7 1.3 fusion.17
  96.0 0.0 copy-start.2
  96.0 0.1 copy.30
  96.1 1.5 broadcast_in_dim.167
  97.6 3.9 %all-to-all-start.1 = ((bf16[16,1,512,128]{2,3,1,0:T(8,128)(2,1)}), bf16[16,1,512,128]{2,3,1,0:T(8,128)(2,1)S(1)}, u32[]{:S(2)}, u32[]{:S(2)}) async-start(bf16[16,1,512,128]{2,3,1,0:T(8,128)(2,1)} %broadcast_in_dim.167), calls=%async_computation.1 | async-start | bytes 4194304 | tf_op jit(solution)/shard_map/all_to_all | solution.py:28
  101.5 0.0 all-gather.3.cloned.1.call-start
  101.6 0.0 collective-permute-done
  101.7 1.2 fusion.40
  102.9 0.0 all-gather.3.cloned.1.call-update
  103.0 53.5 %all-to-all-done.1 = bf16[16,1,512,128]{2,3,1,0:T(8,128)(2,1)S(1)} async-done(((bf16[16,1,512,128]{2,3,1,0:T(8,128)(2,1)}), bf16[16,1,512,128]{2,3,1,0:T(8,128)(2,1)S(1)}, u32[]{:S(2)}, u32[]{:S(2)}) %all-to-all-start.1) | async-done | bytes 2097184 | tf_op jit(solution)/shard_map/all_to_all | solution.py:28
  156.4 0.8 fusion.7
  157.2 0.4 copy.40
  157.6 0.5 broadcast.1945
  158.1 2.3 %reduce.3 = bf16[512,256]{1,0:T(8,128)(2,1)S(1)} reduce(bf16[512,1,256]{2,1,0:T(2,128)(2,1)S(1)} %bitcast.65, bf16[]{:T(256)} %broadcast.1945), dimensions={1}, to_apply=%bitcast.60.reduce_sub_computation | reduce | bytes 524290
  160.4 0.8 reshape.278
  161.2 9.5 %all-to-all-start.2 = ((bf16[32,2,2048]{2,1,0:T(2,128)(2,1)}), bf16[32,2,2048]{2,1,0:T(2,128)(2,1)S(1)}, u32[]{:S(2)}, u32[]{:S(2)}) async-start(bf16[32,2,2048]{2,1,0:T(2,128)(2,1)} %reshape.278), calls=%async_computation.2 | async-start | bytes 524288 | tf_op jit(solution)/shard_map/all_to_all | solution.py:108
  170.7 0.1 copy.33
  170.9 0.0 all-gather.3.cloned.1.call-done
  170.9 3.3 %convolution_convert_fusion.1 = bf16[512,256]{1,0:T(8,128)(2,1)} fusion(bf16[512,2048]{1,0:T(8,128)(2,1)} %all-gather.3.cloned.1.call-done, bf16[2048,256]{1,0:T(8,128)(2,1)} %param.10), kind=kOutput, calls=%fused_computation.11 | convolution fusion | flops 537001984 | bytes 3407872 | tf_op jit(solution)/shard_map/dot_general | solution.py:78
  174.2 7.0 %all-to-all-done.2 = bf16[32,2,2048]{2,1,0:T(2,128)(2,1)S(1)} async-done(((bf16[32,2,2048]{2,1,0:T(2,128)(2,1)}), bf16[32,2,2048]{2,1,0:T(2,128)(2,1)S(1)}, u32[]{:S(2)}, u32[]{:S(2)}) %all-to-all-start.2) | async-done | bytes 262176 | tf_op jit(solution)/shard_map/all_to_all | solution.py:108
  181.1 0.3 reshape.279
  181.5 1.2 gather_fusion.1
  182.6 0.1 reshape.249
  182.7 1.0 multiply_reduce_fusion
  (33 shorter events, 0.4 us)
Async XLA Ops:
  7.2 149.3 %copy-start = (bf16[1,2048,256]{2,1,0:T(8,128)(2,1)S(1)}, bf16[1,2048,256]{2,1,0:T(8,128)(2,1)}, u32[]{:S(2)}) copy-start(bf16[1,2048,256]{2,1,0:T(8,128)(2,1)} %param.17) | copy-start | bytes 3145732
  7.2 86.1 %copy-start.6 = (f32[4096]{0:T(1024)S(1)}, f32[4096]{0:T(1024)}, u32[]{:S(2)}) copy-start(f32[4096]{0:T(1024)} %param.14) | copy-start | bytes 49156
  7.2 86.1 %copy-start.4 = (bf16[1,4096,128]{2,1,0:T(8,128)(2,1)S(1)}, bf16[1,4096,128]{2,1,0:T(8,128)(2,1)}, u32[]{:S(2)}) copy-start(bf16[1,4096,128]{2,1,0:T(8,128)(2,1)} %param.15) | copy-start | bytes 3145732
  7.2 82.8 %all-gather.5.cloned.1.call-start = ((), (), s32[]{:S(2)}) async-start(), calls=%async_computation.4 | async-start | bytes 4456448 | tf_op jit(solution)/shard_map/all_gather | solution.py:95
  40.4 61.3 %collective-permute-start = (bf16[15,128]{1,0:T(8,128)(2,1)S(1)}, bf16[15,128]{1,0:T(8,128)(2,1)S(1)}, u32[]{:S(2)}, u32[]{:S(2)}) collective-permute-start(bf16[15,128]{1,0:T(8,128)(2,1)S(1)} %slice.58), channel_id=1, source_target_pairs={{0,16},{16,32},{32,48},{48,64},{64,80},{80,96},{96,112},{112,128},... | collective-permute-start | bytes 11528 | tf_op jit(solution)/shard_map/ppermute | solution.py:17
  90.0 3.4 %copy-start.1 = (bf16[1,512,4096]{2,1,0:T(8,128)(2,1)S(1)}, bf16[1,512,4096]{2,1,0:T(8,128)(2,1)}, u32[]{:S(2)}) copy-start(bf16[1,512,4096]{2,1,0:T(8,128)(2,1)} %all-gather.5.cloned.1.call-done) | copy-start | bytes 12582916
  93.2 1.5 copy-start.5
  96.0 5.7 %copy-start.2 = (bf16[512,128]{1,0:T(8,128)(2,1)S(1)}, bf16[512,128]{1,0:T(8,128)(2,1)}, u32[]{:S(2)}) copy-start(bf16[512,128]{1,0:T(8,128)(2,1)} %param.9) | copy-start | bytes 393220
  97.6 5.3 %copy-start.3 = (f32[128,2]{0,1:T(2,128)S(1)}, f32[128,2]{0,1:T(2,128)}, u32[]{:S(2)}) copy-start(f32[128,2]{0,1:T(2,128)} %param.13) | copy-start | bytes 3076
  97.6 58.8 %all-to-all-start.1 = ((bf16[16,1,512,128]{2,3,1,0:T(8,128)(2,1)}), bf16[16,1,512,128]{2,3,1,0:T(8,128)(2,1)S(1)}, u32[]{:S(2)}, u32[]{:S(2)}) async-start(bf16[16,1,512,128]{2,3,1,0:T(8,128)(2,1)} %broadcast_in_dim.167), calls=%async_computation.1 | async-start | bytes 4194304 | tf_op jit(solution)/shard_map/all_to_all | solution.py:28
  101.5 69.4 %all-gather.3.cloned.1.call-start = ((), (), s32[]{:S(2)}) async-start(), calls=%async_computation.3 | async-start | bytes 2228224 | tf_op jit(solution)/shard_map/all_gather | solution.py:79
  161.2 19.9 %all-to-all-start.2 = ((bf16[32,2,2048]{2,1,0:T(2,128)(2,1)}), bf16[32,2,2048]{2,1,0:T(2,128)(2,1)S(1)}, u32[]{:S(2)}, u32[]{:S(2)}) async-start(bf16[32,2,2048]{2,1,0:T(2,128)(2,1)} %reshape.278), calls=%async_computation.2 | async-start | bytes 524288 | tf_op jit(solution)/shard_map/all_to_all | solution.py:108
Sparse Core Ops, SparseCore 0:
  39.8 50.1 all-gather.4
  105.0 63.7 all-gather.2
where the time goes:
time: 192 us; the launch traced here: 191 us
  waiting for transfers between devices  108 us (56%)
  blocking collectives  24.9 us (13%)
  starting transfers between devices  15.6 us (8%)
  between operations  14.3 us (7%)
  local copies, waits for them, and re-layouts  11.8 us (6%)
  other arithmetic  9.6 us (5%)
  matrix products  6.55 us (3%)
    all_to_all x1, waiting for transfers between devices, copy_for_each(): lax.all_to_all(jnp.broadcast_to(value[None], (size, *value.shape)), axis,...  53.5 us
    all_gather x1, waiting for transfers between devices, shards(): portion = lax.all_gather(arrived, 'tp', axis=2, tiled=True)  47.3 us
    all_to_all x1, blocking collectives, shards(): lax.all_to_all(outgoing, 'ep', split_axis=0, concat_axis=1, tiled=True)  24.9 us
    all_to_all x1, starting transfers between devices, shards(): lax.all_to_all(produced, 'ep', split_axis=1, concat_axis=0, tiled=True)  9.53 us
    all_to_all x1, waiting for transfers between devices, shards(): lax.all_to_all(produced, 'ep', split_axis=1, concat_axis=0, tiled=True)  6.97 us
    all_to_all x1, starting transfers between devices, copy_for_each(): lax.all_to_all(jnp.broadcast_to(value[None], (size, *value.shape)), axis,...  3.91 us
  transfers between devices with their start and end apart: 5, of which 3 were waited for; matrix products, arithmetic and copies ran while one was open for 9% of the time, Pallas kernels for 0%

commit v1 on v0

v1 whole, which is shorter than its diff:
```python
import functools

import jax
import jax.numpy as jnp
from jax import lax
from jax.experimental import pallas as pl
from jax.experimental.pallas import tpu as pltpu
from jax.sharding import PartitionSpec as P

MESH = pl.DeviceIdType.MESH
F32, BF16 = jnp.float32, jnp.bfloat16
norm_eps = 1e-06


def dot(a, b):
    return jnp.dot(a, b, preferred_element_type=F32)


def kernel(
    n_ep,
    n_x,
    n_tp,
    mix_in,
    mix_w,
    x_in,
    idx_in,
    share_in,
    gain_in,
    gate_w,
    up_w,
    down_w,
    mix_out,
    exp_out,
    X,
    H,
    M,
    W,
    D,
    MW,
    xin,
    mixin,
    halo,
    idx_v,
    share_v,
    gain_v,
    OUT,
    RET,
    Y,
    acc,
    sq,
    share_hi,
    share_lo,
    mixo,
    expo,
    ld_sem,
    st_sem,
    ring_send,
    ici,
    d2d,
    disp_send,
    disp_recv,
    ret_send,
    ret_recv,
    halo_sem,
):
    n_z = n_ep // n_x
    ny = n_tp // 2
    half_ring = ny // 2
    ep, t = lax.axis_index("ep"), lax.axis_index("tp")
    z, x = ep // n_x, ep % n_x
    y, core = t // 2, t % 2
    sibling = 2 * y + (1 - core)
    right = 2 * ((y + 1) % ny) + core
    left = 2 * ((y + ny - 1) % ny) + core
    cap = OUT.shape[0] // n_ep
    slots = OUT.shape[0]
    half = slots // 2
    tok = xin.shape[0]
    feat = xin.shape[1]
    ch = mixin.shape[1]
    mrows = mixo.shape[0]
    hid = H.shape[2]
    width = n_tp * feat

    def offset(k):
        i = k // n_x
        dz = jnp.where(i % 2 == 1, (i + 1) // 2, (n_z - i // 2) % n_z)
        return dz, k % n_x

    def source(k):
        dz, dx = offset(k)
        return ((z + dz) % n_z) * n_x + (x + dx) % n_x

    def target(k):
        dz, dx = offset(k)
        return ((z + n_z - dz) % n_z) * n_x + (x + n_x - dx) % n_x

    loads = [
        (idx_in, idx_v),
        (x_in, xin),
        (mix_in, mixin.at[pl.ds(16, mrows)]),
        (share_in, share_v),
        (gain_in, gain_v),
        (gate_w.at[0], W.at[:, pl.ds(0, hid)]),
        (up_w.at[0], W.at[:, pl.ds(hid, hid)]),
        (down_w.at[0], D),
        (mix_w, MW),
    ]
    loads = [pltpu.make_async_copy(a, b, ld_sem.at[i]) for i, (a, b) in enumerate(loads)]
    for copy in loads:
        copy.start()

    barrier = pltpu.get_barrier_semaphore()

    def greet(k, carry):
        pl.semaphore_signal(barrier, inc=1, device_id=(target(k), t), device_id_type=MESH)
        return carry

    for peer in (sibling, right, left):
        pl.semaphore_signal(barrier, inc=1, device_id=(ep, peer), device_id_type=MESH)
    lax.fori_loop(1, n_ep, greet, 0)

    loads[0].wait()
    first, second = idx_v[0:1, :], idx_v[1:2, :]
    experts = lax.broadcasted_iota(jnp.int32, (128, tok), 0)
    named = [(experts == row).astype(F32).astype(BF16) for row in (first, second)]
    before = lax.broadcasted_iota(jnp.int32, (tok, tok), 0) < lax.broadcasted_iota(
        jnp.int32, (tok, tok), 1
    )
    both = named[0] + named[1]
    counts = dot(both, before.astype(F32).astype(BF16)).astype(BF16)
    slot = lax.broadcasted_iota(jnp.int32, (slots, 128), 0)
    owner = lax.broadcasted_iota(jnp.int32, (slots, 128), 1)
    spread = (slot // cap == owner).astype(F32).astype(BF16)
    place = (lax.broadcasted_iota(jnp.int32, (slots, tok), 0) % cap).astype(F32)
    hit = dot(spread, counts) == place
    picks = [
        jnp.where(jnp.logical_and(hit, dot(spread, row) > 0.5), 1.0, 0.0) for row in named
    ]
    loads[1].wait()
    OUT[...] = dot((picks[0] + picks[1]).astype(BF16), xin[...]).astype(BF16)

    loads[2].wait()
    window = lax.shift_left(jnp.int32(2), t // (n_tp // 4))

    def pooled(ext, first_pos):
        total = ext
        for step in (1, 2, 4, 8):
            shifted = pltpu.roll(total, step, 0)
            total = jnp.where(window > step, total + shifted, total)
        rows = ext.shape[0]
        pos = lax.broadcasted_iota(jnp.int32, (rows, ch), 0) + (first_pos - 16)
        div = jnp.minimum(jnp.maximum(pos + 1, 1), window).astype(F32)
        return (total / div - ext)[16:].astype(BF16)

    mixin[0:16, :] = jnp.zeros((16, ch), BF16)
    M[t] = pooled(mixin[...].astype(F32), ep * mrows)
    acc[...] = jnp.zeros(acc.shape, F32)
    sq[...] = jnp.zeros(sq.shape, F32)

    pl.semaphore_wait(barrier, n_ep + 2)

    halo_copy = pltpu.make_async_remote_copy(
        src_ref=mixin.at[pl.ds(mrows, 16)],
        dst_ref=halo,
        send_sem=halo_sem.at[0],
        recv_sem=halo_sem.at[1],
        device_id=((ep + 1) % n_ep, t),
        device_id_type=MESH,
    )
    halo_copy.start()

    def ring(rid, buf, base, rows, nq):
        cr = rows // nq

        def chunk(block, q):
            return buf.at[block, pl.ds(base + q * cr, cr)]

        def push(block, q, peer, recv):
            pltpu.make_async_remote_copy(
                src_ref=chunk(block, q),
                dst_ref=chunk(block, q),
                send_sem=ring_send.at[rid],
                recv_sem=recv,
                device_id=(ep, peer),
                device_id_type=MESH,
            ).start()

        def arrived(block, q, recv):
            pltpu.make_async_remote_copy(
                src_ref=chunk(block, q),
                dst_ref=chunk(block, q),
                send_sem=ring_send.at[rid],
                recv_sem=recv,
                device_id=(ep, sibling),
                device_id_type=MESH,
            ).wait_recv()

        def begin(qs):
            for q in qs:
                if half_ring > 1 or q % 2 == 0:
                    push(t, q, right, ici.at[rid, 1, q])
                if half_ring > 1 or q % 2 == 1:
                    push(t, q, left, ici.at[rid, ny - 1, q])
            for q in qs:
                push(t, q, sibling, d2d.at[rid, 0, q])

        def step(s):
            for q in range(nq):
                if s < half_ring or q % 2 == 0:
                    block = 2 * ((y + ny - s) % ny) + core
                    arrived(block, q, ici.at[rid, s, q])
                    if s + 1 < half_ring or (s + 1 == half_ring and q % 2 == 0):
                        push(block, q, right, ici.at[rid, s + 1, q])
                    push(block, q, sibling, d2d.at[rid, s, q])
                if s < half_ring or q % 2 == 1:
                    block = 2 * ((y + s) % ny) + core
                    arrived(block, q, ici.at[rid, ny - s, q])
                    if s + 1 < half_ring or (s + 1 == half_ring and q % 2 == 1):
                        push(block, q, left, ici.at[rid, ny - s - 1, q])
                    push(block, q, sibling, d2d.at[rid, ny - s, q])

        def from_sibling(rel):
            block = 2 * ((y + ny - rel) % ny) + (1 - core)
            for q in range(nq):
                arrived(block, q, d2d.at[rid, rel, q])

        def drain():
            whole = buf.at[pl.ds(0, n_tp - 1), pl.ds(base, rows)]
            pltpu.make_async_remote_copy(
                src_ref=whole,
                dst_ref=whole,
                send_sem=ring_send.at[rid],
                recv_sem=ici.at[rid, 1, 0],
                device_id=(ep, sibling),
                device_id_type=MESH,
            ).wait_send()

        return begin, step, from_sibling, drain

    nqm, nqx, nqh = 4, 2, 2
    m_ring = ring(0, M, 0, mrows, nqm)
    x_rings = [ring(1 + h, X, h * half, half, nqx) for h in (0, 1)]
    h_rings = [ring(3 + h, H, h * half, half, nqh) for h in (0, 1)]

    m_ring[0](range(1, nqm))

    def dispatch(h):
        def send(k, carry):
            to = target(k)
            pltpu.make_async_remote_copy(
                src_ref=OUT.at[pl.ds(pl.multiple_of(to * cap, cap), cap)],
                dst_ref=X.at[t, pl.ds(pl.multiple_of(k * cap, cap), cap)],
                send_sem=disp_send,
                recv_sem=disp_recv.at[h],
                device_id=(to, t),
                device_id_type=MESH,
            ).start()
            return carry

        lax.fori_loop(max(1, h * (n_ep // 2)), (h + 1) * (n_ep // 2), send, 0)

    dispatch(0)
    dispatch(1)
    X[t, pl.ds(0, cap)] = OUT[pl.ds(pl.multiple_of(ep * cap, cap), cap)]

    def dispatched(h):
        rows = X.at[t, pl.ds(cap, half - cap)] if h == 0 else X.at[t, pl.ds(half, half)]
        pltpu.make_async_remote_copy(
            src_ref=rows,
            dst_ref=rows,
            send_sem=disp_send,
            recv_sem=disp_recv.at[h],
            device_id=(ep, sibling),
            device_id_type=MESH,
        ).wait_recv()

    halo_copy.wait_recv()
    past = jnp.where(ep > 0, halo[...].astype(F32), 0.0)
    head = jnp.concatenate([past, mixin[16:32, :].astype(F32)], axis=0)
    M[t, 0:16] = pooled(head, ep * mrows)
    m_ring[0](range(0, 1))

    loads[3].wait()
    s0, s1 = share_v[0:1, :], share_v[1:2, :]
    total = s0 + s1
    weights = picks[0] * (s0 / total) + picks[1] * (s1 / total)
    high = weights.astype(BF16)
    share_hi[...] = high.astype(F32).T.astype(BF16)
    share_lo[...] = (weights - high.astype(F32)).T.astype(BF16)

    m_ring[1](1)
    for copy in loads[4:]:
        copy.wait()

    tile = min(128, half)

    def gather_unit(h, rel):
        x_rings[h][2](rel)
        chip = (y + ny - rel) % ny
        cols = pl.ds(pl.multiple_of(chip * 2 * feat, 2 * feat), 2 * feat)

        def body(i, carry):
            rows = pl.ds(pl.multiple_of(h * half + i * tile, tile), tile)
            value = jnp.concatenate([X[2 * chip, rows], X[2 * chip + 1, rows]], axis=1)
            value = value.astype(F32)
            scaled = (value * gain_v[:, cols]).astype(BF16)
            acc[rows, :] += dot(scaled, W[cols, :])
            square = value * value
            part = square[:, 0:128]
            for j in range(1, 2 * feat // 128):
                part += square[:, j * 128 : (j + 1) * 128]
            sq[rows, :] += part
            return carry

        lax.fori_loop(0, half // tile, body, 0)

    def gather_half(h, then):
        for s in range(1, half_ring):
            x_rings[h][1](s)
            if s == half_ring - 1:
                then()
            if s == 1:
                gather_unit(h, 0)
            else:
                gather_unit(h, s - 1)
                gather_unit(h, ny - s + 1)
        x_rings[h][1](half_ring)
        gather_unit(h, half_ring - 1)
        gather_unit(h, ny - half_ring + 1)
        gather_unit(h, half_ring)

    def activate(h):
        def body(i, carry):
            rows = pl.ds(pl.multiple_of(h * half + i * tile, tile), tile)
            inverse = lax.rsqrt(jnp.sum(sq[rows, :], axis=1, keepdims=True) / width + norm_eps)
            gate = acc[rows, 0:hid] * inverse
            up = acc[rows, hid : 2 * hid] * inverse
            H[t, rows] = (gate / (1.0 + jnp.exp(-gate)) * up).astype(BF16)
            return carry

        lax.fori_loop(0, half // tile, body, 0)

    def project(blocks, rows, weight):
        total = None
        for i in range(0, n_tp, 2):
            value = jnp.concatenate([blocks[i, rows], blocks[i + 1, rows]], axis=1)
            depth = value.shape[1]
            term = dot(value, weight[(i // 2) * depth : (i // 2 + 1) * depth, :])
            total = term if total is None else total + term
        return total.astype(BF16)

    def hidden_half(h, then):
        for s in range(1, half_ring):
            h_rings[h][1](s)
            if s == half_ring - 1:
                then()
        h_rings[h][1](half_ring)
        for rel in range(ny):
            h_rings[h][2](rel)

        def body(i, carry):
            rows = pl.ds(pl.multiple_of(h * half + i * tile, tile), tile)
            Y[rows, :] = project(H, rows, D)
            return carry

        lax.fori_loop(0, half // tile, body, 0)

        def send(k, carry):
            pltpu.make_async_remote_copy(
                src_ref=Y.at[pl.ds(pl.multiple_of(k * cap, cap), cap)],
                dst_ref=RET.at[pl.ds(pl.multiple_of(ep * cap, cap), cap)],
                send_sem=ret_send,
                recv_sem=ret_recv,
                device_id=(source(k), t),
                device_id_type=MESH,
            ).start()
            return carry

        lax.fori_loop(max(1, h * (n_ep // 2)), (h + 1) * (n_ep // 2), send, 0)

    def start_far():
        dispatched(1)
        x_rings[1][0](range(nqx))

    def start_hidden_near():
        activate(0)
        h_rings[0][0](range(nqh))

    def start_hidden_far():
        pass

    dispatched(0)
    x_rings[0][0](range(nqx))
    gather_half(0, start_far)
    gather_half(1, start_hidden_near)
    activate(1)
    h_rings[1][0](range(nqh))
    hidden_half(0, start_hidden_far)
    hidden_half(1, start_hidden_far)

    for s in range(2, half_ring + 1):
        m_ring[1](s)
    for rel in range(ny):
        m_ring[2](rel)

    def mix_tile(i, carry):
        rows = pl.ds(pl.multiple_of(i * 128, 128), 128)
        mixo[rows, :] = project(M, rows, MW)
        return carry

    lax.fori_loop(0, mrows // 128, mix_tile, 0)
    mix_store = pltpu.make_async_copy(mixo, mix_out, st_sem.at[0])
    mix_store.start()

    RET[pl.ds(pl.multiple_of(ep * cap, cap), cap)] = Y[0:cap]
    back = RET.at[pl.ds(0, slots - cap)]
    pltpu.make_async_remote_copy(
        src_ref=back,
        dst_ref=back,
        send_sem=ret_send,
        recv_sem=ret_recv,
        device_id=(ep, sibling),
        device_id_type=MESH,
    ).wait_recv()
    expo[...] = (dot(share_hi[...], RET[...]) + dot(share_lo[...], RET[...])).astype(BF16)
    exp_store = pltpu.make_async_copy(expo, exp_out, st_sem.at[1])
    exp_store.start()

    halo_copy.wait_send()
    for r in [m_ring, *x_rings, *h_rings]:
        r[3]()
    for buf, sem in ((OUT, disp_send), (Y, ret_send)):
        rows = buf.at[pl.ds(0, slots - cap)]
        pltpu.make_async_remote_copy(
            src_ref=rows,
            dst_ref=rows,
            send_sem=sem,
            recv_sem=ret_recv,
            device_id=(ep, sibling),
            device_id_type=MESH,
        ).wait_send()
    mix_store.wait()
    exp_store.wait()


def shards(
    n_ep,
    n_tp,
    mix_input,
    mix_weight,
    expert_input,
    expert_index,
    route_share,
    norm_gain,
    gate_weight,
    up_weight,
    down_weight,
):
    mrows, ch = mix_input.shape
    cols = mix_weight.shape[1]
    tok, feat = expert_input.shape
    hid = gate_weight.shape[2]
    out_feat = down_weight.shape[2]
    width = norm_gain.shape[0]
    n_x = 4 if n_ep % 4 == 0 else 1
    slots = 2 * tok * expert_index.shape[1]
    ny = n_tp // 2
    dma = pltpu.SemaphoreType.DMA
    anywhere = pl.BlockSpec(memory_space=pl.ANY)
    return pl.pallas_call(
        functools.partial(kernel, n_ep, n_x, n_tp),
        out_shape=(
            jax.ShapeDtypeStruct((mrows, cols), BF16),
            jax.ShapeDtypeStruct((tok, out_feat), BF16),
        ),
        in_specs=[anywhere] * 9,
        out_specs=(anywhere, anywhere),
        scratch_shapes=[
            pltpu.VMEM((n_tp, slots, feat), BF16),
            pltpu.VMEM((n_tp, slots, hid), BF16),
            pltpu.VMEM((n_tp, mrows, ch), BF16),
            pltpu.VMEM((width, 2 * hid), BF16),
            pltpu.VMEM((n_tp * hid, out_feat), BF16),
            pltpu.VMEM((n_tp * ch, cols), BF16),
            pltpu.VMEM((tok, feat), BF16),
            pltpu.VMEM((mrows + 16, ch), BF16),
            pltpu.VMEM((16, ch), BF16),
            pltpu.VMEM((2, tok), jnp.int32),
            pltpu.VMEM((2, tok), F32),
            pltpu.VMEM((1, width), F32),
            pltpu.VMEM((slots, feat), BF16),
            pltpu.VMEM((slots, out_feat), BF16),
            pltpu.VMEM((slots, out_feat), BF16),
            pltpu.VMEM((slots, 2 * hid), F32),
            pltpu.VMEM((slots, 128), F32),
            pltpu.VMEM((tok, slots), BF16),
            pltpu.VMEM((tok, slots), BF16),
            pltpu.VMEM((mrows, cols), BF16),
            pltpu.VMEM((tok, out_feat), BF16),
            dma((9,)),
            dma((2,)),
            dma((5,)),
            dma((5, ny, 4)),
            dma((5, ny, 4)),
            dma,
            dma((2,)),
            dma,
            dma,
            dma((2,)),
        ],
        compiler_params=pltpu.CompilerParams(
            collective_id=0, has_side_effects=True, vmem_limit_bytes=48 * 2**20
        ),
    )(
        mix_input,
        mix_weight,
        expert_input,
        expert_index.T,
        route_share.T,
        norm_gain.reshape(1, width),
        gate_weight,
        up_weight,
        down_weight,
    )


def solution(mesh):
    placed = (
        P("ep", "tp"),
        P(None, "tp"),
        P("ep", "tp"),
        P("ep", None),
        P("ep", None),
        P(),
        P("ep", None, "tp"),
        P("ep", None, "tp"),
        P("ep", None, "tp"),
    )
    return jax.shard_map(
        functools.partial(shards, mesh.shape["ep"], mesh.shape["tp"]),
        mesh=mesh,
        in_specs=placed,
        out_specs=(P("ep", "tp"), P("ep", "tp")),
        check_vma=False,
    )
```

time: 192 us -> 109 us (0.57)
  waiting for transfers between devices: 108 us -> 0 us
  Pallas kernels: 0 us -> 98.9 us
  blocking collectives: 24.9 us -> 0 us
  starting transfers between devices: 15.6 us -> 0 us
  between operations: 14.3 us -> 0.67 us
  other arithmetic: 9.6 us -> 0 us
  matrix products: 6.55 us -> 0 us
  local copies, waits for them, and re-layouts: 11.8 us -> 9.37 us
    pallas_call x0 -> x1, Pallas kernels: none -> 98.9 us  [shards(): pl.pallas_call(functools.partial(kernel, n_ep, n_x, n_tp), out_shape=(jax...]
    all_to_all x2 -> x0, waiting for transfers between devices: 60.4 us -> none  [the longest x1 53.5 us: copy_for_each(): lax.all_to_all(jnp.broadcast_to(value[None], (size, *value.shape)), axis,...]
    all_gather x2 -> x0, waiting for transfers between devices: 47.3 us -> none  [the longest x1 47.3 us: shards(): portion = lax.all_gather(arrived, 'tp', axis=2, tiled=True)]
    all_to_all x1 -> x0, blocking collectives: 24.9 us -> none  [shards(): lax.all_to_all(outgoing, 'ep', split_axis=0, concat_axis=1, tiled=True)]
    all_to_all x2 -> x0, starting transfers between devices: 13.4 us -> none  [the longest x1 9.53 us: shards(): lax.all_to_all(produced, 'ep', split_axis=1, concat_axis=0, tiled=True)]
    unnamed x19 -> x20, local copies, waits for them, and re-layouts: 2.62 us -> 9.37 us
    dot_general x4 -> x0, matrix products: 6.55 us -> none  [the longest x1 3.27 us: shards(): jnp.dot(lax.all_gather(pooled, 'tp', axis=1, tiled=True), mix_weight, pre...]
    reduce_sum x4 -> x0, other arithmetic: 4.38 us -> none  [the longest x1 3.23 us: shards(): squares = jnp.sum(jnp.square(portion.astype(jnp.float32)), axis=2)]
  transfers between devices with their start and end apart: 5 -> 0, of which waited for: 3 -> 0; matrix products, arithmetic and copies ran while one was open for 9% -> 0% of each run, Pallas kernels for 0% -> 0%
where the time goes in v1:
time: 109 us
  Pallas kernels  98.9 us (91%)
  local copies, waits for them, and re-layouts  9.37 us (9%)
    pallas_call x1, Pallas kernels, shards(): pl.pallas_call(functools.partial(kernel, n_ep, n_x, n_tp), out_shape=(jax...  98.9 us
    unnamed x20, local copies, waits for them, and re-layouts  9.37 us

profile of v1, /device:TPU:1, one launch (start us, length us, event | category | flops | bytes accessed | tf_op | source)
XLA Modules:
  0.0 108.9 jit_solution(1886403539981598241)
XLA Ops:
  0.6 0.0 copy-start.8
  0.6 0.0 copy-start.7
  0.7 0.7 copy-done.8
  1.3 0.0 copy-done.7
  1.3 0.0 copy-start
  1.3 1.2 %copy-done = bf16[2048,256]{1,0:T(8,128)(2,1)S(1)} copy-done((bf16[2048,256]{1,0:T(8,128)(2,1)S(1)}, bf16[2048,256]{1,0:T(8,128)(2,1)}, u32[]{:S(2)}) %copy-start) | copy-done | bytes 1048600
  2.6 0.0 copy-start.1
  2.6 1.2 %copy-done.1 = bf16[1,4096,128]{2,1,0:T(8,128)(2,1)S(1)} copy-done((bf16[1,4096,128]{2,1,0:T(8,128)(2,1)S(1)}, bf16[1,4096,128]{2,1,0:T(8,128)(2,1)}, u32[]{:S(2)}) %copy-start.1) | copy-done | bytes 1048600
  3.8 0.0 copy-start.2
  3.8 1.2 %copy-done.2 = bf16[1,4096,128]{2,1,0:T(8,128)(2,1)S(1)} copy-done((bf16[1,4096,128]{2,1,0:T(8,128)(2,1)S(1)}, bf16[1,4096,128]{2,1,0:T(8,128)(2,1)}, u32[]{:S(2)}) %copy-start.2) | copy-done | bytes 1048600
  5.0 0.0 copy-start.3
  5.0 1.2 %copy-done.3 = bf16[1,2048,256]{2,1,0:T(8,128)(2,1)S(1)} copy-done((bf16[1,2048,256]{2,1,0:T(8,128)(2,1)S(1)}, bf16[1,2048,256]{2,1,0:T(8,128)(2,1)}, u32[]{:S(2)}) %copy-start.3) | copy-done | bytes 1048600
  6.2 0.0 copy-start.4
  6.2 0.9 copy-done.4
  7.1 0.0 copy-start.5
  7.1 0.8 copy-done.5
  8.0 0.0 copy-start.6
  8.0 0.7 copy-done.6
  8.7 98.9 %shard_map.104 = (bf16[512,256]{1,0:T(8,128)(2,1)S(1)}, bf16[128,256]{1,0:T(8,128)(2,1)S(1)}) custom-call(bf16[512,128]{1,0:T(8,128)(2,1)S(1)} %copy-done.4, bf16[2048,256]{1,0:T(8,128)(2,1)S(1)} %copy-done, bf16[128,256]{1,0:T(8,128)(2,1)S(1)} %copy-done.5, s32[2,128]{1,0:T(2,128)S(1)} %bitcast.4, f32[2,128]{1,0:T(2,128)S(1)} %bitcast.5, ...), custom_call_target="tpu_custom_call" | custom-call | tf_op jit(solution)/shard_map/pallas_call | solution.py:471
  107.6 0.7 copy.13
  108.3 0.6 copy.14
Async XLA Ops:
  0.6 0.7 copy-start.8
  0.6 0.7 copy-start.7
  1.3 1.2 %copy-start = (bf16[2048,256]{1,0:T(8,128)(2,1)S(1)}, bf16[2048,256]{1,0:T(8,128)(2,1)}, u32[]{:S(2)}) copy-start(bf16[2048,256]{1,0:T(8,128)(2,1)} %mix_w.1) | copy-start | bytes 3145732
  2.6 1.2 %copy-start.1 = (bf16[1,4096,128]{2,1,0:T(8,128)(2,1)S(1)}, bf16[1,4096,128]{2,1,0:T(8,128)(2,1)}, u32[]{:S(2)}) copy-start(bf16[1,4096,128]{2,1,0:T(8,128)(2,1)} %gate_w.1) | copy-start | bytes 3145732
  3.8 1.2 %copy-start.2 = (bf16[1,4096,128]{2,1,0:T(8,128)(2,1)S(1)}, bf16[1,4096,128]{2,1,0:T(8,128)(2,1)}, u32[]{:S(2)}) copy-start(bf16[1,4096,128]{2,1,0:T(8,128)(2,1)} %up_w.1) | copy-start | bytes 3145732
  5.0 1.2 %copy-start.3 = (bf16[1,2048,256]{2,1,0:T(8,128)(2,1)S(1)}, bf16[1,2048,256]{2,1,0:T(8,128)(2,1)}, u32[]{:S(2)}) copy-start(bf16[1,2048,256]{2,1,0:T(8,128)(2,1)} %down_w.1) | copy-start | bytes 3145732
  6.2 0.9 copy-start.4
  7.1 0.8 copy-start.5
  8.0 0.7 copy-start.6

commit v2 on v1

v2 whole, which is shorter than its diff:
```python
import functools

import jax
import jax.numpy as jnp
from jax import lax
from jax.experimental import pallas as pl
from jax.experimental.pallas import tpu as pltpu
from jax.sharding import PartitionSpec as P

MESH = pl.DeviceIdType.MESH
F32, BF16 = jnp.float32, jnp.bfloat16
norm_eps = 1e-06


def dot(a, b):
    return jnp.dot(a, b, preferred_element_type=F32)


def kernel(
    n_ep,
    n_x,
    n_tp,
    mix_in,
    mix_w,
    x_in,
    idx_in,
    share_in,
    gain_in,
    gate_w,
    up_w,
    down_w,
    mix_out,
    exp_out,
    X,
    H,
    M,
    W,
    D,
    MW,
    xin,
    mixin,
    halo,
    idx_v,
    share_v,
    gain_v,
    OUT,
    RET,
    Y,
    acc,
    sq,
    share_hi,
    share_lo,
    mixo,
    expo,
    ld_sem,
    st_sem,
    ring_send,
    ici,
    d2d,
    disp_send,
    disp_recv,
    ret_send,
    ret_recv,
    halo_sem,
):
    n_z = n_ep // n_x
    ny = n_tp // 2
    half_ring = ny // 2
    ep, t = lax.axis_index("ep"), lax.axis_index("tp")
    z, x = ep // n_x, ep % n_x
    y, core = t // 2, t % 2
    sibling = 2 * y + (1 - core)
    right = 2 * ((y + 1) % ny) + core
    left = 2 * ((y + ny - 1) % ny) + core
    cap = OUT.shape[0] // n_ep
    slots = OUT.shape[0]
    half = slots // 2
    tok = xin.shape[0]
    feat = xin.shape[1]
    ch = mixin.shape[1]
    mrows = mixo.shape[0]
    hid = H.shape[2]
    width = n_tp * feat

    def offset(k):
        i = k // n_x
        return ((i + 1) // 2 if i % 2 else (n_z - i // 2) % n_z), k % n_x

    def source(k):
        dz, dx = offset(k)
        return lax.rem(z + dz, n_z) * n_x + lax.rem(x + dx, n_x)

    def target(k):
        dz, dx = offset(k)
        return lax.rem(z + n_z - dz, n_z) * n_x + lax.rem(x + n_x - dx, n_x)

    loads = [
        (idx_in, idx_v),
        (x_in, xin),
        (mix_in, mixin.at[pl.ds(16, mrows)]),
        (share_in, share_v),
        (gain_in, gain_v),
        (gate_w.at[0], W.at[:, pl.ds(0, hid)]),
        (up_w.at[0], W.at[:, pl.ds(hid, hid)]),
        (down_w.at[0], D),
        (mix_w, MW),
    ]
    loads = [pltpu.make_async_copy(a, b, ld_sem.at[i]) for i, (a, b) in enumerate(loads)]
    for copy in loads:
        copy.start()

    barrier = pltpu.get_barrier_semaphore()

    for k in range(n_ep - 1, 0, -1):
        pl.semaphore_signal(barrier, inc=1, device_id=(target(k), t), device_id_type=MESH)
    for peer in (sibling, right, left):
        pl.semaphore_signal(barrier, inc=1, device_id=(ep, peer), device_id_type=MESH)

    with jax.named_scope("l0"):
        loads[0].wait()
    first, second = idx_v[0:1, :], idx_v[1:2, :]
    experts = lax.broadcasted_iota(jnp.int32, (128, tok), 0)
    named = [(experts == row).astype(F32).astype(BF16) for row in (first, second)]
    before = lax.broadcasted_iota(jnp.int32, (tok, tok), 0) < lax.broadcasted_iota(
        jnp.int32, (tok, tok), 1
    )
    both = named[0] + named[1]
    counts = dot(both, before.astype(F32).astype(BF16)).astype(BF16)
    slot = lax.broadcasted_iota(jnp.int32, (slots, 128), 0)
    owner = lax.broadcasted_iota(jnp.int32, (slots, 128), 1)
    spread = (slot // cap == owner).astype(F32).astype(BF16)
    place = (lax.broadcasted_iota(jnp.int32, (slots, tok), 0) % cap).astype(F32)
    hit = dot(spread, counts) == place
    picks = [
        jnp.where(jnp.logical_and(hit, dot(spread, row) > 0.5), 1.0, 0.0) for row in named
    ]
    with jax.named_scope("l1"):
        loads[1].wait()
    OUT[...] = dot((picks[0] + picks[1]).astype(BF16), xin[...]).astype(BF16)

    with jax.named_scope("l2"):
        loads[2].wait()
    window = lax.shift_left(jnp.int32(2), t // (n_tp // 4))

    def pooled(ext, first_pos):
        total = ext
        for step in (1, 2, 4, 8):
            shifted = pltpu.roll(total, step, 0)
            total = jnp.where(window > step, total + shifted, total)
        rows = ext.shape[0]
        pos = lax.broadcasted_iota(jnp.int32, (rows, ch), 0) + (first_pos - 16)
        div = jnp.minimum(jnp.maximum(pos + 1, 1), window).astype(F32)
        return (total / div - ext)[16:].astype(BF16)

    mixin[0:16, :] = jnp.zeros((16, ch), BF16)
    M[t] = pooled(mixin[...].astype(F32), ep * mrows)
    acc[...] = jnp.zeros(acc.shape, F32)
    sq[...] = jnp.zeros(sq.shape, F32)

    with jax.named_scope("bar"):
        pl.semaphore_wait(barrier, n_ep + 2)

    halo_copy = pltpu.make_async_remote_copy(
        src_ref=mixin.at[pl.ds(mrows, 16)],
        dst_ref=halo,
        send_sem=halo_sem.at[0],
        recv_sem=halo_sem.at[1],
        device_id=((ep + 1) % n_ep, t),
        device_id_type=MESH,
    )
    halo_copy.start()

    def ring(rid, buf, rows, nq):
        cr = rows // nq

        def chunk(block, q):
            return buf.at[block, pl.ds(q * cr, cr)]

        def push(block, q, peer, recv):
            pltpu.make_async_remote_copy(
                src_ref=chunk(block, q),
                dst_ref=chunk(block, q),
                send_sem=ring_send.at[rid],
                recv_sem=recv,
                device_id=(ep, peer),
                device_id_type=MESH,
            ).start()

        def arrived(block, q, recv):
            pltpu.make_async_remote_copy(
                src_ref=chunk(block, q),
                dst_ref=chunk(block, q),
                send_sem=ring_send.at[rid],
                recv_sem=recv,
                device_id=(ep, sibling),
                device_id_type=MESH,
            ).wait_recv()

        def begin(q):
            push(t, q, right, ici.at[rid, 1, q])
            push(t, q, left, ici.at[rid, ny - 1, q])
            push(t, q, sibling, d2d.at[rid, 0, q])

        def step(s, q):
            if s < half_ring or q % 2 == 0:
                block = 2 * lax.rem(y + ny - s, ny) + core
                arrived(block, q, ici.at[rid, s, q])
                if s + 1 < half_ring or (s + 1 == half_ring and q % 2 == 0):
                    push(block, q, right, ici.at[rid, s + 1, q])
                push(block, q, sibling, d2d.at[rid, s, q])
            if s < half_ring or q % 2 == 1:
                block = 2 * lax.rem(y + s, ny) + core
                arrived(block, q, ici.at[rid, ny - s, q])
                if s + 1 < half_ring or (s + 1 == half_ring and q % 2 == 1):
                    push(block, q, left, ici.at[rid, ny - s - 1, q])
                push(block, q, sibling, d2d.at[rid, ny - s, q])

        def from_sibling(rel, q):
            block = 2 * lax.rem(y + ny - rel, ny) + (1 - core)
            arrived(block, q, d2d.at[rid, rel, q])

        def drain():
            whole = buf.at[pl.ds(0, n_tp - 1)]
            pltpu.make_async_remote_copy(
                src_ref=whole,
                dst_ref=whole,
                send_sem=ring_send.at[rid],
                recv_sem=ici.at[rid, 1, 0],
                device_id=(ep, sibling),
                device_id_type=MESH,
            ).wait_send()

        return begin, step, from_sibling, drain

    nq = 4
    m_ring = ring(0, M, mrows, nq)
    x_ring = ring(1, X, slots, nq)
    h_ring = ring(2, H, slots, nq)

    def dispatch(h):
        for k in range(max(1, h * (n_ep // 2)), (h + 1) * (n_ep // 2)):
            to = target(k)
            pltpu.make_async_remote_copy(
                src_ref=OUT.at[pl.ds(pl.multiple_of(to * cap, cap), cap)],
                dst_ref=X.at[t, pl.ds(k * cap, cap)],
                send_sem=disp_send,
                recv_sem=disp_recv.at[h],
                device_id=(to, t),
                device_id_type=MESH,
            ).start()

    with jax.named_scope("dispatch"):
        dispatch(0)
        dispatch(1)
    for q in range(1, nq):
        m_ring[0](q)
    X[t, pl.ds(0, cap)] = OUT[pl.ds(pl.multiple_of(ep * cap, cap), cap)]

    def dispatched(h):
        rows = X.at[t, pl.ds(cap, half - cap)] if h == 0 else X.at[t, pl.ds(half, half)]
        pltpu.make_async_remote_copy(
            src_ref=rows,
            dst_ref=rows,
            send_sem=disp_send,
            recv_sem=disp_recv.at[h],
            device_id=(ep, sibling),
            device_id_type=MESH,
        ).wait_recv()

    loads[3].wait()
    s0, s1 = share_v[0:1, :], share_v[1:2, :]
    total = s0 + s1
    weights = picks[0] * (s0 / total) + picks[1] * (s1 / total)
    high = weights.astype(BF16)
    share_hi[...] = high.astype(F32).T.astype(BF16)
    share_lo[...] = (weights - high.astype(F32)).T.astype(BF16)

    with jax.named_scope("halo"):
        halo_copy.wait_recv()
    past = jnp.where(ep > 0, halo[...].astype(F32), 0.0)
    head = jnp.concatenate([past, mixin[16:32, :].astype(F32)], axis=0)
    M[t, 0:16] = pooled(head, ep * mrows)
    m_ring[0](0)

    with jax.named_scope("m1"):
        for q in range(1, nq):
            m_ring[1](1, q)
    with jax.named_scope("disp0"):
        dispatched(0)
    for q in range(nq // 2):
        x_ring[0](q)
    with jax.named_scope("m10"):
        m_ring[1](1, 0)
    with jax.named_scope("disp1"):
        dispatched(1)
    for q in range(nq // 2, nq):
        x_ring[0](q)
    for copy in loads[4:]:
        copy.wait()

    tile = slots // nq

    def gather_tile(rel, q):
        x_ring[2](rel, q)
        chip = lax.rem(y + ny - rel, ny)
        cols = pl.ds(pl.multiple_of(chip * 2 * feat, 2 * feat), 2 * feat)
        rows = pl.ds(q * tile, tile)
        value = jnp.concatenate([X[2 * chip, rows], X[2 * chip + 1, rows]], axis=1)
        value = value.astype(F32)
        scaled = (value * gain_v[:, cols]).astype(BF16)
        acc[rows, :] += dot(scaled, W[cols, :])
        square = value * value
        part = square[:, 0:128]
        for j in range(1, 2 * feat // 128):
            part += square[:, j * 128 : (j + 1) * 128]
        sq[rows, :] += part

    def activate(q):
        rows = pl.ds(q * tile, tile)
        inverse = lax.rsqrt(jnp.sum(sq[rows, :], axis=1, keepdims=True) / width + norm_eps)
        gate = acc[rows, 0:hid] * inverse
        up = acc[rows, hid : 2 * hid] * inverse
        H[t, rows] = (gate / (1.0 + jnp.exp(-gate)) * up).astype(BF16)
        acc[rows, :] = jnp.zeros((tile, 2 * hid), F32)

    def down_tile(rel, q):
        h_ring[2](rel, q)
        chip = lax.rem(y + ny - rel, ny)
        cols = pl.ds(pl.multiple_of(chip * 2 * hid, 2 * hid), 2 * hid)
        rows = pl.ds(q * tile, tile)
        value = jnp.concatenate([H[2 * chip, rows], H[2 * chip + 1, rows]], axis=1)
        acc[rows, :] += dot(value, D[cols, :])

    def project(blocks, rows, weight):
        total = None
        for i in range(0, n_tp, 2):
            value = jnp.concatenate([blocks[i, rows], blocks[i + 1, rows]], axis=1)
            depth = value.shape[1]
            term = dot(value, weight[(i // 2) * depth : (i // 2 + 1) * depth, :])
            total = term if total is None else total + term
        return total.astype(BF16)

    def tiles_at(tile_of, distance, q):
        tile_of(distance, q)
        if distance > 0:
            tile_of(ny - distance, q)

    def travel(name, ring, tile_of, woven, between, finish):
        for s in range(1, half_ring):
            with jax.named_scope(f"{name}{s}"):
                if woven:
                    for q in range(nq):
                        ring[1](s, q)
                        tiles_at(tile_of, s - 1, q)
                else:
                    for q in range(nq):
                        ring[1](s, q)
                    for q in range(nq):
                        tiles_at(tile_of, s - 1, q)
        with jax.named_scope(f"{name}b"):
            between()
            for q in range(nq):
                tiles_at(tile_of, half_ring - 1, q)
        with jax.named_scope(f"{name}{half_ring}"):
            for q in range(nq):
                ring[1](half_ring, q)
        with jax.named_scope(f"{name}end"):
            for q in range(nq):
                tile_of(half_ring, q)
                finish(q)

    def begin_hidden(q):
        activate(q)
        h_ring[0](q)

    def mixer(s):
        for q in (*range(1, nq), 0):
            m_ring[1](s, q)

    def give_back(q):
        rows = pl.ds(q * tile, tile)
        Y[rows, :] = acc[rows, :].astype(BF16)
        per = n_ep // nq
        for k in range(max(1, q * per), (q + 1) * per):
            pltpu.make_async_remote_copy(
                src_ref=Y.at[pl.ds(k * cap, cap)],
                dst_ref=RET.at[pl.ds(pl.multiple_of(ep * cap, cap), cap)],
                send_sem=ret_send,
                recv_sem=ret_recv,
                device_id=(source(k), t),
                device_id_type=MESH,
            ).start()

    travel("x", x_ring, gather_tile, True, lambda: None, begin_hidden)
    travel("h", h_ring, down_tile, False, lambda: mixer(2), give_back)
    with jax.named_scope("mrest"):
        for s in range(3, half_ring + 1):
            mixer(s)

    for rel in range(ny):
        for q in range(nq):
            m_ring[2](rel, q)

    def mix_tile(i, carry):
        rows = pl.ds(pl.multiple_of(i * 128, 128), 128)
        mixo[rows, :] = project(M, rows, MW)
        return carry

    with jax.named_scope("mixdot"):
        lax.fori_loop(0, mrows // 128, mix_tile, 0)
    mix_store = pltpu.make_async_copy(mixo, mix_out, st_sem.at[0])
    mix_store.start()

    RET[pl.ds(pl.multiple_of(ep * cap, cap), cap)] = Y[0:cap]
    back = RET.at[pl.ds(0, slots - cap)]
    with jax.named_scope("retwait"):
        pltpu.make_async_remote_copy(
            src_ref=back,
            dst_ref=back,
            send_sem=ret_send,
            recv_sem=ret_recv,
            device_id=(ep, sibling),
            device_id_type=MESH,
        ).wait_recv()
    with jax.named_scope("combine"):
        expo[...] = (dot(share_hi[...], RET[...]) + dot(share_lo[...], RET[...])).astype(BF16)
    exp_store = pltpu.make_async_copy(expo, exp_out, st_sem.at[1])
    exp_store.start()

    with jax.named_scope("drain"):
        halo_copy.wait_send()
        for r in (m_ring, x_ring, h_ring):
            r[3]()
        for buf, sem in ((OUT, disp_send), (Y, ret_send)):
            rows = buf.at[pl.ds(0, slots - cap)]
            pltpu.make_async_remote_copy(
                src_ref=rows,
                dst_ref=rows,
                send_sem=sem,
                recv_sem=ret_recv,
                device_id=(ep, sibling),
                device_id_type=MESH,
            ).wait_send()
        mix_store.wait()
        exp_store.wait()


def shards(
    n_ep,
    n_tp,
    mix_input,
    mix_weight,
    expert_input,
    expert_index,
    route_share,
    norm_gain,
    gate_weight,
    up_weight,
    down_weight,
):
    mrows, ch = mix_input.shape
    cols = mix_weight.shape[1]
    tok, feat = expert_input.shape
    hid = gate_weight.shape[2]
    out_feat = down_weight.shape[2]
    width = norm_gain.shape[0]
    n_x = 4 if n_ep % 4 == 0 else 1
    slots = 2 * tok * expert_index.shape[1]
    ny = n_tp // 2
    dma = pltpu.SemaphoreType.DMA
    anywhere = pl.BlockSpec(memory_space=pl.ANY)
    return pl.pallas_call(
        functools.partial(kernel, n_ep, n_x, n_tp),
        out_shape=(
            jax.ShapeDtypeStruct((mrows, cols), BF16),
            jax.ShapeDtypeStruct((tok, out_feat), BF16),
        ),
        in_specs=[anywhere] * 9,
        out_specs=(anywhere, anywhere),
        scratch_shapes=[
            pltpu.VMEM((n_tp, slots, feat), BF16),
            pltpu.VMEM((n_tp, slots, hid), BF16),
            pltpu.VMEM((n_tp, mrows, ch), BF16),
            pltpu.VMEM((width, 2 * hid), BF16),
            pltpu.VMEM((n_tp * hid, out_feat), BF16),
            pltpu.VMEM((n_tp * ch, cols), BF16),
            pltpu.VMEM((tok, feat), BF16),
            pltpu.VMEM((mrows + 16, ch), BF16),
            pltpu.VMEM((16, ch), BF16),
            pltpu.VMEM((2, tok), jnp.int32),
            pltpu.VMEM((2, tok), F32),
            pltpu.VMEM((1, width), F32),
            pltpu.VMEM((slots, feat), BF16),
            pltpu.VMEM((slots, out_feat), BF16),
            pltpu.VMEM((slots, out_feat), BF16),
            pltpu.VMEM((slots, 2 * hid), F32),
            pltpu.VMEM((slots, 128), F32),
            pltpu.VMEM((tok, slots), BF16),
            pltpu.VMEM((tok, slots), BF16),
            pltpu.VMEM((mrows, cols), BF16),
            pltpu.VMEM((tok, out_feat), BF16),
            dma((9,)),
            dma((2,)),
            dma((3,)),
            dma((3, ny, 4)),
            dma((3, ny, 4)),
            dma,
            dma((2,)),
            dma,
            dma,
            dma((2,)),
        ],
        compiler_params=pltpu.CompilerParams(
            collective_id=0, has_side_effects=True, vmem_limit_bytes=67043328
        ),
    )(
        mix_input,
        mix_weight,
        expert_input,
        expert_index.T,
        route_share.T,
        norm_gain.reshape(1, width),
        gate_weight,
        up_weight,
        down_weight,
    )


def solution(mesh):
    placed = (
        P("ep", "tp"),
        P(None, "tp"),
        P("ep", "tp"),
        P("ep", None),
        P("ep", None),
        P(),
        P("ep", None, "tp"),
        P("ep", None, "tp"),
        P("ep", None, "tp"),
    )
    return jax.shard_map(
        functools.partial(shards, mesh.shape["ep"], mesh.shape["tp"]),
        mesh=mesh,
        in_specs=placed,
        out_specs=(P("ep", "tp"), P("ep", "tp")),
        check_vma=False,
    )
```

time: 109 us -> 75.9 us (0.70)
  Pallas kernels: 98.9 us -> 72.1 us
  local copies, waits for them, and re-layouts: 9.37 us -> 2.33 us
    pallas_call x1, Pallas kernels: 98.9 us -> 72.1 us  [shards(): pl.pallas_call(functools.partial(kernel, n_ep, n_x, n_tp), out_shape=(jax...]
    unnamed x20 -> x4, local copies, waits for them, and re-layouts: 9.37 us -> 2.33 us
where the time goes in v2:
time: 75.9 us; the launch traced here: 75.1 us
  Pallas kernels  72.1 us (95%)
  local copies, waits for them, and re-layouts  2.33 us (3%)
    pallas_call x1, Pallas kernels, shards(): pl.pallas_call(functools.partial(kernel, n_ep, n_x, n_tp), out_shape=(jax...  72.1 us
    unnamed x4, local copies, waits for them, and re-layouts  2.33 us

profile of v2, /device:TPU:1, one launch (start us, length us, event | category | flops | bytes accessed | tf_op | source)
XLA Modules:
  0.0 75.1 jit_solution(11657693119185722592)
XLA Ops:
  0.6 72.1 %shard_map.104 = (bf16[512,256]{1,0:T(8,128)(2,1)}, bf16[128,256]{1,0:T(8,128)(2,1)}) custom-call(bf16[512,128]{1,0:T(8,128)(2,1)} %mix_in.1, bf16[2048,256]{1,0:T(8,128)(2,1)} %mix_w.1, bf16[128,256]{1,0:T(8,128)(2,1)} %x_in.1, s32[2,128]{1,0:T(2,128)} %bitcast.4, f32[2,128]{1,0:T(2,128)} %bitcast.5, f32[1,4096]{1,0:T(1,128)} %bitcast.3, ...), custom_call_target="tpu_custom_call" | custom-call | tf_op jit(solution)/shard_map/pallas_call | solution.py:472
  72.8 0.0 copy-start
  72.8 1.7 %copy.13 = bf16[512,256]{1,0:T(8,128)(2,1)} copy(bf16[512,256]{1,0:T(8,128)(2,1)} %get-tuple-element.4) | data formatting | bytes 524288
  74.5 0.0 copy-done
  74.5 0.6 copy.14
Async XLA Ops:
  72.8 1.7 %copy-start = (bf16[128,256]{1,0:T(8,128)(2,1)S(1)}, bf16[128,256]{1,0:T(8,128)(2,1)}, u32[]{:S(2)}) copy-start(bf16[128,256]{1,0:T(8,128)(2,1)} %get-tuple-element.5) | copy-start | bytes 196612

commit v3 on v2

--- a/solution.py
+++ b/solution.py
@@ -50,13 +50,12 @@
     sq,
     share_hi,
     share_lo,
-    mixo,
-    expo,
     ld_sem,
-    st_sem,
     ring_send,
     ici,
     d2d,
+    m_ici,
+    m_d2d,
     disp_send,
     disp_recv,
     ret_send,
@@ -72,13 +71,15 @@
     sibling = 2 * y + (1 - core)
     right = 2 * ((y + 1) % ny) + core
     left = 2 * ((y + ny - 1) % ny) + core
+    right2 = 2 * ((y + 2) % ny) + core
+    left2 = 2 * ((y + ny - 2) % ny) + core
     cap = OUT.shape[0] // n_ep
     slots = OUT.shape[0]
     half = slots // 2
     tok = xin.shape[0]
     feat = xin.shape[1]
     ch = mixin.shape[1]
-    mrows = mixo.shape[0]
+    mrows = mix_out.shape[0]
     hid = H.shape[2]
     width = n_tp * feat
 
@@ -93,6 +94,14 @@
     def target(k):
         dz, dx = offset(k)
         return lax.rem(z + n_z - dz, n_z) * n_x + lax.rem(x + n_x - dx, n_x)
+
+    barrier = pltpu.get_barrier_semaphore()
+
+    for k in range(n_ep - 1, 0, -1):
+        pl.semaphore_signal(barrier, inc=1, device_id=(target(k), t), device_id_type=MESH)
+    near = (sibling, right, left, right2, left2) if ny > 4 else (sibling, right, left)
+    for peer in near:
+        pl.semaphore_signal(barrier, inc=1, device_id=(ep, peer), device_id_type=MESH)
 
     loads = [
         (idx_in, idx_v),
@@ -108,13 +117,6 @@
     loads = [pltpu.make_async_copy(a, b, ld_sem.at[i]) for i, (a, b) in enumerate(loads)]
     for copy in loads:
         copy.start()
-
-    barrier = pltpu.get_barrier_semaphore()
-
-    for k in range(n_ep - 1, 0, -1):
-        pl.semaphore_signal(barrier, inc=1, device_id=(target(k), t), device_id_type=MESH)
-    for peer in (sibling, right, left):
-        pl.semaphore_signal(barrier, inc=1, device_id=(ep, peer), device_id_type=MESH)
 
     with jax.named_scope("l0"):
         loads[0].wait()
@@ -158,7 +160,7 @@
     sq[...] = jnp.zeros(sq.shape, F32)
 
     with jax.named_scope("bar"):
-        pl.semaphore_wait(barrier, n_ep + 2)
+        pl.semaphore_wait(barrier, n_ep - 1 + len(near))
 
     halo_copy = pltpu.make_async_remote_copy(
         src_ref=mixin.at[pl.ds(mrows, 16)],
@@ -170,11 +172,17 @@
     )
     halo_copy.start()
 
-    def ring(rid, buf, rows, nq):
+    def ring(rid, buf, rows, nq, skip, ici, d2d):
         cr = rows // nq
 
         def chunk(block, q):
             return buf.at[block, pl.ds(q * cr, cr)]
+
+        def landed(rel, q):
+            return ici.at[rel - 1, q]
+
+        def handed(rel, q):
+            return d2d.at[0 if rid == 0 else ny + q if rel == half_ring else rel]
 
         def push(block, q, peer, recv):
             pltpu.make_async_remote_copy(
@@ -186,10 +194,10 @@
                 device_id_type=MESH,
             ).start()
 
-        def arrived(block, q, recv):
+        def arrived(ref, recv):
             pltpu.make_async_remote_copy(
-                src_ref=chunk(block, q),
-                dst_ref=chunk(block, q),
+                src_ref=ref,
+                dst_ref=ref,
                 send_sem=ring_send.at[rid],
                 recv_sem=recv,
                 device_id=(ep, sibling),
@@ -197,27 +205,41 @@
             ).wait_recv()
 
         def begin(q):
-            push(t, q, right, ici.at[rid, 1, q])
-            push(t, q, left, ici.at[rid, ny - 1, q])
-            push(t, q, sibling, d2d.at[rid, 0, q])
+            push(t, q, right, landed(1, q))
+            push(t, q, left, landed(ny - 1, q))
+            push(t, q, sibling, handed(0, q))
+
+        skip = skip if half_ring > 2 else ()
+        seen = set()
 
         def step(s, q):
             if s < half_ring or q % 2 == 0:
                 block = 2 * lax.rem(y + ny - s, ny) + core
-                arrived(block, q, ici.at[rid, s, q])
-                if s + 1 < half_ring or (s + 1 == half_ring and q % 2 == 0):
-                    push(block, q, right, ici.at[rid, s + 1, q])
-                push(block, q, sibling, d2d.at[rid, s, q])
+                arrived(chunk(block, q), landed(s, q))
+                if s + 1 < half_ring or (s + 1 == half_ring and q % 2 == 0 and q not in skip):
+                    push(block, q, right, landed(s + 1, q))
+                if q in skip and s + 2 == half_ring and q % 2 == 0:
+                    push(block, q, right2, landed(s + 2, q))
+                push(block, q, sibling, handed(s, q))
             if s < half_ring or q % 2 == 1:
                 block = 2 * lax.rem(y + s, ny) + core
-                arrived(block, q, ici.at[rid, ny - s, q])
-                if s + 1 < half_ring or (s + 1 == half_ring and q % 2 == 1):
-                    push(block, q, left, ici.at[rid, ny - s - 1, q])
-                push(block, q, sibling, d2d.at[rid, ny - s, q])
+                arrived(chunk(block, q), landed(ny - s, q))
+                if s + 1 < half_ring or (s + 1 == half_ring and q % 2 == 1 and q not in skip):
+                    push(block, q, left, landed(ny - s - 1, q))
+                if q in skip and s + 2 == half_ring and q % 2 == 1:
+                    push(block, q, left2, landed(ny - s - 2, q))
+                push(block, q, sibling, handed(ny - s, q))
 
         def from_sibling(rel, q):
             block = 2 * lax.rem(y + ny - rel, ny) + (1 - core)
-            arrived(block, q, d2d.at[rid, rel, q])
+            if rel == half_ring:
+                arrived(chunk(block, q), handed(rel, q))
+            elif rel not in seen:
+                seen.add(rel)
+                arrived(buf.at[block], handed(rel, q))
+
+        def all_from_sibling():
+            arrived(buf.at[pl.ds(0, ny)], handed(0, 0))
 
         def drain():
             whole = buf.at[pl.ds(0, n_tp - 1)]
@@ -225,44 +247,40 @@
                 src_ref=whole,
                 dst_ref=whole,
                 send_sem=ring_send.at[rid],
-                recv_sem=ici.at[rid, 1, 0],
+                recv_sem=ici.at[0, 0],
                 device_id=(ep, sibling),
                 device_id_type=MESH,
             ).wait_send()
 
-        return begin, step, from_sibling, drain
+        return begin, step, from_sibling, drain, all_from_sibling
 
     nq = 4
-    m_ring = ring(0, M, mrows, nq)
-    x_ring = ring(1, X, slots, nq)
-    h_ring = ring(2, H, slots, nq)
-
-    def dispatch(h):
-        for k in range(max(1, h * (n_ep // 2)), (h + 1) * (n_ep // 2)):
-            to = target(k)
-            pltpu.make_async_remote_copy(
-                src_ref=OUT.at[pl.ds(pl.multiple_of(to * cap, cap), cap)],
-                dst_ref=X.at[t, pl.ds(k * cap, cap)],
-                send_sem=disp_send,
-                recv_sem=disp_recv.at[h],
-                device_id=(to, t),
-                device_id_type=MESH,
-            ).start()
-
-    with jax.named_scope("dispatch"):
-        dispatch(0)
-        dispatch(1)
-    for q in range(1, nq):
-        m_ring[0](q)
+    m_ring = ring(0, M, mrows, 2, (0, 1), m_ici, m_d2d)
+    x_ring = ring(1, X, slots, nq, (), ici.at[0], d2d.at[0])
+    h_ring = ring(2, H, slots, nq, (2, 3), ici.at[1], d2d.at[1])
+
+    per = n_ep // nq
+    for k in range(1, n_ep):
+        to = target(k)
+        pltpu.make_async_remote_copy(
+            src_ref=OUT.at[pl.ds(pl.multiple_of(to * cap, cap), cap)],
+            dst_ref=X.at[t, pl.ds(k * cap, cap)],
+            send_sem=disp_send,
+            recv_sem=disp_recv.at[k // per],
+            device_id=(to, t),
+            device_id_type=MESH,
+        ).start()
+    m_ring[0](1)
     X[t, pl.ds(0, cap)] = OUT[pl.ds(pl.multiple_of(ep * cap, cap), cap)]
 
-    def dispatched(h):
-        rows = X.at[t, pl.ds(cap, half - cap)] if h == 0 else X.at[t, pl.ds(half, half)]
+    def dispatched(q):
+        first = max(1, q * per)
+        rows = X.at[t, pl.ds(first * cap, ((q + 1) * per - first) * cap)]
         pltpu.make_async_remote_copy(
             src_ref=rows,
             dst_ref=rows,
             send_sem=disp_send,
-            recv_sem=disp_recv.at[h],
+            recv_sem=disp_recv.at[q],
             device_id=(ep, sibling),
             device_id_type=MESH,
         ).wait_recv()
@@ -282,19 +300,6 @@
     M[t, 0:16] = pooled(head, ep * mrows)
     m_ring[0](0)
 
-    with jax.named_scope("m1"):
-        for q in range(1, nq):
-            m_ring[1](1, q)
-    with jax.named_scope("disp0"):
-        dispatched(0)
-    for q in range(nq // 2):
-        x_ring[0](q)
-    with jax.named_scope("m10"):
-        m_ring[1](1, 0)
-    with jax.named_scope("disp1"):
-        dispatched(1)
-    for q in range(nq // 2, nq):
-        x_ring[0](q)
     for copy in loads[4:]:
         copy.wait()
 
@@ -345,42 +350,60 @@
         if distance > 0:
             tile_of(ny - distance, q)
 
-    def travel(name, ring, tile_of, woven, between, finish):
+    def travel(name, ring, tile_of, first, woven, between, finish):
         for s in range(1, half_ring):
             with jax.named_scope(f"{name}{s}"):
-                if woven:
-                    for q in range(nq):
-                        ring[1](s, q)
+                for q in range(nq):
+                    if s == 1:
+                        first(q)
+                    ring[1](s, q)
+                    if woven and s > 1:
                         tiles_at(tile_of, s - 1, q)
-                else:
-                    for q in range(nq):
-                        ring[1](s, q)
+                between(s)
+                if not woven or s == 1:
                     for q in range(nq):
                         tiles_at(tile_of, s - 1, q)
         with jax.named_scope(f"{name}b"):
-            between()
             for q in range(nq):
-                tiles_at(tile_of, half_ring - 1, q)
-        with jax.named_scope(f"{name}{half_ring}"):
-            for q in range(nq):
-                ring[1](half_ring, q)
-        with jax.named_scope(f"{name}end"):
-            for q in range(nq):
-                tile_of(half_ring, q)
-                finish(q)
+                if woven:
+                    tiles_at(tile_of, half_ring - 1, q)
+        for group in ((0, 1, 2, 3),) if woven else ((2, 3), (0, 1)):
+            with jax.named_scope(f"{name}{half_ring}"):
+                for q in group:
+                    ring[1](half_ring, q)
+            with jax.named_scope(f"{name}end"):
+                for q in group:
+                    if not woven:
+                        tiles_at(tile_of, half_ring - 1, q)
+                for q in group:
+                    tile_of(half_ring, q)
+                    finish(q)
 
     def begin_hidden(q):
         activate(q)
         h_ring[0](q)
 
-    def mixer(s):
-        for q in (*range(1, nq), 0):
-            m_ring[1](s, q)
+    mixer_steps = [(s, q) for s in range(1, half_ring + 1) for q in (1, 0)]
+
+    def mixer():
+        s, q = mixer_steps.pop(0)
+        m_ring[1](s, q)
+
+    ahead = 2
+
+    def enter(q):
+        if q == 0:
+            with jax.named_scope("m11"):
+                mixer()
+        for p in range(ahead + 1) if q == 0 else range(q + ahead, q + ahead + 1):
+            if p < nq:
+                with jax.named_scope(f"disp{p}"):
+                    dispatched(p)
+                x_ring[0](p)
 
     def give_back(q):
         rows = pl.ds(q * tile, tile)
         Y[rows, :] = acc[rows, :].astype(BF16)
-        per = n_ep // nq
         for k in range(max(1, q * per), (q + 1) * per):
             pltpu.make_async_remote_copy(
                 src_ref=Y.at[pl.ds(k * cap, cap)],
@@ -391,25 +414,30 @@
                 device_id_type=MESH,
             ).start()
 
-    travel("x", x_ring, gather_tile, True, lambda: None, begin_hidden)
-    travel("h", h_ring, down_tile, False, lambda: mixer(2), give_back)
+    def after_rows(s):
+        if s == half_ring - 1:
+            mixer()
+
+    def after_hidden(s):
+        if s == half_ring - 1:
+            mixer()
+            mixer()
+
+    travel("x", x_ring, gather_tile, enter, True, after_rows, begin_hidden)
+    travel("h", h_ring, down_tile, lambda q: None, False, after_hidden, give_back)
     with jax.named_scope("mrest"):
-        for s in range(3, half_ring + 1):
-            mixer(s)
-
-    for rel in range(ny):
-        for q in range(nq):
-            m_ring[2](rel, q)
+        while mixer_steps:
+            mixer()
+
+    m_ring[4]()
 
     def mix_tile(i, carry):
         rows = pl.ds(pl.multiple_of(i * 128, 128), 128)
-        mixo[rows, :] = project(M, rows, MW)
+        mix_out[rows, :] = project(M, rows, MW)
         return carry
 
     with jax.named_scope("mixdot"):
         lax.fori_loop(0, mrows // 128, mix_tile, 0)
-    mix_store = pltpu.make_async_copy(mixo, mix_out, st_sem.at[0])
-    mix_store.start()
 
     RET[pl.ds(pl.multiple_of(ep * cap, cap), cap)] = Y[0:cap]
     back = RET.at[pl.ds(0, slots - cap)]
@@ -423,9 +451,7 @@
             device_id_type=MESH,
         ).wait_recv()
     with jax.named_scope("combine"):
-        expo[...] = (dot(share_hi[...], RET[...]) + dot(share_lo[...], RET[...])).astype(BF16)
-    exp_store = pltpu.make_async_copy(expo, exp_out, st_sem.at[1])
-    exp_store.start()
+        exp_out[...] = (dot(share_hi[...], RET[...]) + dot(share_lo[...], RET[...])).astype(BF16)
 
     with jax.named_scope("drain"):
         halo_copy.wait_send()
@@ -441,8 +467,6 @@
                 device_id=(ep, sibling),
                 device_id_type=MESH,
             ).wait_send()
-        mix_store.wait()
-        exp_store.wait()
 
 
 def shards(
@@ -472,11 +496,11 @@
     return pl.pallas_call(
         functools.partial(kernel, n_ep, n_x, n_tp),
         out_shape=(
-            jax.ShapeDtypeStruct((mrows, cols), BF16),
-            jax.ShapeDtypeStruct((tok, out_feat), BF16),
+            pltpu.VMEM((mrows, cols), BF16),
+            pltpu.VMEM((tok, out_feat), BF16),
         ),
         in_specs=[anywhere] * 9,
-        out_specs=(anywhere, anywhere),
+        out_specs=(pl.BlockSpec(memory_space=pltpu.VMEM),) * 2,
         scratch_shapes=[
             pltpu.VMEM((n_tp, slots, feat), BF16),
             pltpu.VMEM((n_tp, slots, hid), BF16),
@@ -497,21 +521,20 @@
             pltpu.VMEM((slots, 128), F32),
             pltpu.VMEM((tok, slots), BF16),
             pltpu.VMEM((tok, slots), BF16),
-            pltpu.VMEM((mrows, cols), BF16),
-            pltpu.VMEM((tok, out_feat), BF16),
             dma((9,)),
-            dma((2,)),
             dma((3,)),
-            dma((3, ny, 4)),
-            dma((3, ny, 4)),
+            dma((2, ny - 1, 4)),
+            dma((2, ny + 4)),
+            dma((ny - 1, 2)),
+            dma((1,)),
             dma,
-            dma((2,)),
+            dma((4,)),
             dma,
             dma,
             dma((2,)),
         ],
         compiler_params=pltpu.CompilerParams(
-            collective_id=0, has_side_effects=True, vmem_limit_bytes=67043328
+            collective_id=0, has_side_effects=True, vmem_limit_bytes=60*2**20
         ),
     )(
         mix_input,

time: 75.9 us -> 71.2 us (0.938)
  Pallas kernels: 72.1 us -> 69.1 us
  local copies, waits for them, and re-layouts: 2.33 us -> 1.33 us
    pallas_call x1, Pallas kernels: 72.1 us -> 69.1 us  [shards(): pl.pallas_call(functools.partial(kernel, n_ep, n_x, n_tp), out_shape=(plt...]
    unnamed x4 -> x2, local copies, waits for them, and re-layouts: 2.33 us -> 1.33 us
where the time goes in v3:
time: 71.2 us; the launch traced here: 71.1 us
  Pallas kernels  69.1 us (97%)
  local copies, waits for them, and re-layouts  1.33 us (2%)
    pallas_call x1, Pallas kernels, shards(): pl.pallas_call(functools.partial(kernel, n_ep, n_x, n_tp), out_shape=(plt...  69.1 us

profile of v3, /device:TPU:1, one launch (start us, length us, event | category | flops | bytes accessed | tf_op | source)
XLA Modules:
  0.0 71.1 jit_solution(11343071017149927401)
XLA Ops:
  0.6 69.1 %shard_map.104 = (bf16[512,256]{1,0:T(8,128)(2,1)S(1)}, bf16[128,256]{1,0:T(8,128)(2,1)S(1)}) custom-call(bf16[512,128]{1,0:T(8,128)(2,1)} %mix_in.1, bf16[2048,256]{1,0:T(8,128)(2,1)} %mix_w.1, bf16[128,256]{1,0:T(8,128)(2,1)} %x_in.1, s32[2,128]{1,0:T(2,128)} %bitcast.4, f32[2,128]{1,0:T(2,128)} %bitcast.5, f32[1,4096]{1,0:T(1,128)} %bitcast.3, ...), custom_call_target="tpu_custom_call" | custom-call | tf_op jit(solution)/shard_map/pallas_call | solution.py:496
  69.7 0.7 copy.13
  70.4 0.6 copy.14

commit v4 on v3

--- a/solution.py
+++ b/solution.py
@@ -95,14 +95,6 @@
         dz, dx = offset(k)
         return lax.rem(z + n_z - dz, n_z) * n_x + lax.rem(x + n_x - dx, n_x)
 
-    barrier = pltpu.get_barrier_semaphore()
-
-    for k in range(n_ep - 1, 0, -1):
-        pl.semaphore_signal(barrier, inc=1, device_id=(target(k), t), device_id_type=MESH)
-    near = (sibling, right, left, right2, left2) if ny > 4 else (sibling, right, left)
-    for peer in near:
-        pl.semaphore_signal(barrier, inc=1, device_id=(ep, peer), device_id_type=MESH)
-
     loads = [
         (idx_in, idx_v),
         (x_in, xin),
@@ -115,7 +107,17 @@
         (mix_w, MW),
     ]
     loads = [pltpu.make_async_copy(a, b, ld_sem.at[i]) for i, (a, b) in enumerate(loads)]
-    for copy in loads:
+    for copy in loads[:3]:
+        copy.start()
+
+    barrier = pltpu.get_barrier_semaphore()
+
+    for k in range(n_ep - 1, 0, -1):
+        pl.semaphore_signal(barrier, inc=1, device_id=(target(k), t), device_id_type=MESH)
+    near = (sibling, right, left, right2, left2) if ny > 4 else (sibling, right, left)
+    for peer in near:
+        pl.semaphore_signal(barrier, inc=1, device_id=(ep, peer), device_id_type=MESH)
+    for copy in loads[3:]:
         copy.start()
 
     with jax.named_scope("l0"):
@@ -392,14 +394,14 @@
     ahead = 2
 
     def enter(q):
-        if q == 0:
-            with jax.named_scope("m11"):
-                mixer()
         for p in range(ahead + 1) if q == 0 else range(q + ahead, q + ahead + 1):
             if p < nq:
                 with jax.named_scope(f"disp{p}"):
                     dispatched(p)
                 x_ring[0](p)
+            if p == 0:
+                with jax.named_scope("m11"):
+                    mixer()
 
     def give_back(q):
         rows = pl.ds(q * tile, tile)

time: 71.2 us -> 70.9 us (level)
  no operation moved by 1% of the time
where the time goes in v4:
time: 70.9 us; the launch traced here: 70.7 us
  Pallas kernels  68.7 us (97%)
  local copies, waits for them, and re-layouts  1.33 us (2%)
    pallas_call x1, Pallas kernels, shards(): pl.pallas_call(functools.partial(kernel, n_ep, n_x, n_tp), out_shape=(plt...  68.7 us

profile of v4, /device:TPU:1, one launch (start us, length us, event | category | flops | bytes accessed | tf_op | source)
XLA Modules:
  0.0 70.7 jit_solution(14072968815987183215)
XLA Ops:
  0.6 68.7 %shard_map.104 = (bf16[512,256]{1,0:T(8,128)(2,1)S(1)}, bf16[128,256]{1,0:T(8,128)(2,1)S(1)}) custom-call(bf16[512,128]{1,0:T(8,128)(2,1)} %mix_in.1, bf16[2048,256]{1,0:T(8,128)(2,1)} %mix_w.1, bf16[128,256]{1,0:T(8,128)(2,1)} %x_in.1, s32[2,128]{1,0:T(2,128)} %bitcast.4, f32[2,128]{1,0:T(2,128)} %bitcast.5, f32[1,4096]{1,0:T(1,128)} %bitcast.3, ...), custom_call_target="tpu_custom_call" | custom-call | tf_op jit(solution)/shard_map/pallas_call | solution.py:498
  69.4 0.7 copy.13
  70.1 0.6 copy.14

commit v5 on v4

--- a/solution.py
+++ b/solution.py
@@ -369,7 +369,7 @@
             for q in range(nq):
                 if woven:
                     tiles_at(tile_of, half_ring - 1, q)
-        for group in ((0, 1, 2, 3),) if woven else ((2, 3), (0, 1)):
+        for group in ((0, 1, 2, 3),) if woven else ((3, 2), (1, 0)):
             with jax.named_scope(f"{name}{half_ring}"):
                 for q in group:
                     ring[1](half_ring, q)
@@ -406,7 +406,7 @@
     def give_back(q):
         rows = pl.ds(q * tile, tile)
         Y[rows, :] = acc[rows, :].astype(BF16)
-        for k in range(max(1, q * per), (q + 1) * per):
+        for k in reversed(range(max(1, q * per), (q + 1) * per)):
             pltpu.make_async_remote_copy(
                 src_ref=Y.at[pl.ds(k * cap, cap)],
                 dst_ref=RET.at[pl.ds(pl.multiple_of(ep * cap, cap), cap)],

time: 70.9 us -> 71.6 us (level)
  no operation moved by 1% of the time
where the time goes in v5:
time: 71.6 us; the launch traced here: 71 us
  Pallas kernels  69 us (96%)
  local copies, waits for them, and re-layouts  1.33 us (2%)
    pallas_call x1, Pallas kernels, shards(): pl.pallas_call(functools.partial(kernel, n_ep, n_x, n_tp), out_shape=(plt...  69 us

profile of v5, /device:TPU:1, one launch (start us, length us, event | category | flops | bytes accessed | tf_op | source)
XLA Modules:
  0.0 71.0 jit_solution(8178585659738293264)
XLA Ops:
  0.6 69.0 %shard_map.104 = (bf16[512,256]{1,0:T(8,128)(2,1)S(1)}, bf16[128,256]{1,0:T(8,128)(2,1)S(1)}) custom-call(bf16[512,128]{1,0:T(8,128)(2,1)} %mix_in.1, bf16[2048,256]{1,0:T(8,128)(2,1)} %mix_w.1, bf16[128,256]{1,0:T(8,128)(2,1)} %x_in.1, s32[2,128]{1,0:T(2,128)} %bitcast.4, f32[2,128]{1,0:T(2,128)} %bitcast.5, f32[1,4096]{1,0:T(1,128)} %bitcast.3, ...), custom_call_target="tpu_custom_call" | custom-call | tf_op jit(solution)/shard_map/pallas_call | solution.py:498
  69.6 0.7 copy.13
  70.4 0.6 copy.14
